TPU v7x, 512 devices: a whole 4x4x16 slice. The times are simulated.
512 devices in a mesh: kv: 128 (over z, x, core), tp: 4 (over y).
Axes of the slice: x: 4, y: 4, z: 16, core: 2. Of those that a mesh axis runs over, the one named last changes fastest.
Arguments:
- queries: bfloat16 [16384, 4096], P('kv', 'tp'), may hold values from -6 to 6
- keys: bfloat16 [16384, 512], P('kv', 'tp'), may hold values from -6 to 6
- values: bfloat16 [16384, 512], P('kv', 'tp'), may hold values from -6 to 6
- logsum: float32 [16384, 32], P('kv', 'tp'), may hold values from 2 to 6
- out_grad: bfloat16 [16384, 4096], P('kv', 'tp'), may hold values from -6 to 6
- normed_input: bfloat16 [16384, 4096], P('kv', 'tp'), may hold values from -6 to 6
- chosen: int32 [256, 16], P('kv'), may hold values from 0 to 511, as said below
Outputs:
- query_grad: float32 [16384, 4096], P('kv', 'tp')
- key_grad: float32 [16384, 512], P('kv', 'tp')
- value_grad: float32 [16384, 512], P('kv', 'tp')
- value_weight_grad: float32 [4096, 512], P('kv', 'tp')
Inputs may be any that keep to these rules, and one draw needn't show every extreme that they name: `chosen`: each row r names 16 distinct key blocks, among them block 0 and the blocks r * 2 to r * 2 + 64 / 32 - 1 that hold the query block's own positions. The rows of one device (aligned runs of 2 rows) name at most one block of any other device's 128 / 32 blocks. Blocks after the query block may be named; their keys are masked.
All inputs are finite; a program needn't handle non-finite values.
Results may differ from a plain program's by a relative error of at most 0.008.
Values may be sent and summed in bfloat16 or wider, within the bound.
No kernel may reach another device: no remote copies, remote signals or barrier semaphores. Data moves between devices by JAX's collectives and lax.ppermute only.
A program may use at most 64 MiB of HBM per device.

v0:
```python
import jax
import jax.numpy as jnp
from jax import lax
from jax.sharding import Mesh
from jax.sharding import PartitionSpec as P

HD = 128
QB = 64
KB = 32
NSEL = 16
KV = ("z", "x", "c")
XC = ("x", "c")


def to_peers(parts, axis):
    return lax.all_to_all(parts, axis, split_axis=0, concat_axis=0, tiled=True)


def local(queries, keys, values, logsum, out_grad, normed_input, chosen):
    nz = lax.axis_size("z")
    nq = lax.axis_size(XC)
    tp = lax.axis_size("tp")
    here = lax.axis_index(KV)
    tok = keys.shape[0]
    kblocks = tok // KB
    qblocks = tok // QB
    group = queries.shape[1] // HD
    span = NSEL * KB
    scale = HD ** (-0.5)
    peers = nq * nz
    entries = qblocks * NSEL
    owner = chosen // kblocks
    within = chosen % kblocks
    remote = owner != here
    place = owner % nq * nz + owner // nq
    named = (place[:, :, None] == jnp.arange(peers, dtype=jnp.int32)) & remote[:, :, None]
    wanted = jnp.max(jnp.where(named, within[:, :, None] + 1, 0), axis=(0, 1))
    asked = to_peers(wanted.reshape(nq, nz), XC)
    slot = jnp.where(remote, place, peers + within).reshape(entries)
    taken = jnp.arange(nz, dtype=jnp.int32)[None, :] * kblocks + jnp.maximum(asked - 1, 0)

    def fetch(rows):
        column = lax.all_gather(rows, "z", axis=0, tiled=True).reshape(nz * kblocks, KB, HD)
        got = to_peers(column[taken.reshape(-1)].reshape(nq, nz * KB, HD), XC)
        pool = jnp.concatenate([got.reshape(peers, KB, HD), rows.reshape(kblocks, KB, HD)], axis=0)
        return pool[slot].reshape(qblocks, span, HD)

    onehot = (slot[:, None] == jnp.arange(peers + kblocks, dtype=jnp.int32)[None, :]).astype(
        jnp.float32
    )
    home = ((asked - 1)[:, :, None] == jnp.arange(kblocks, dtype=jnp.int32)).astype(jnp.bfloat16)

    def give_back(part):
        total = jnp.dot(
            onehot.T,
            part.reshape(entries, KB * HD),
            precision=lax.Precision.HIGHEST,
            preferred_element_type=jnp.float32,
        )
        own = total[peers:].reshape(tok, HD)
        sent = total[:peers].astype(jnp.bfloat16).reshape(nq, nz * KB, HD)
        came = to_peers(sent, XC).reshape(nq, nz, KB * HD)
        dense = jnp.einsum("qzk,qze->zke", home, came, preferred_element_type=jnp.float32)
        dense = dense.astype(jnp.bfloat16).reshape(nz, tok, HD)
        sums = to_peers(dense, "z")
        return own + jnp.sum(sums.astype(jnp.float32), axis=0)

    feats = normed_input.shape[1]
    rows_out = feats * tp // peers
    mine = nz // tp
    split = normed_input.reshape(tok, mine, nq, rows_out).transpose(2, 0, 1, 3)
    split = to_peers(split.reshape(nq, tok, mine * rows_out), XC).reshape(nq * tok, mine * rows_out)
    planes = [split]
    for k in range(1, tp):
        planes.append(lax.ppermute(split, "tp", [(i, (i + k) % tp) for i in range(tp)]))
    sel_keys = fetch(keys)
    query_rows = queries.reshape(qblocks, QB, group, HD)
    dout = out_grad.reshape(qblocks, QB, group, HD)
    lse = logsum.reshape(qblocks, QB, group)
    scores = (
        jnp.einsum("bqgd,bjd->bqgj", query_rows, sel_keys, preferred_element_type=jnp.float32)
        * scale
    )
    qpos = here * tok + jnp.arange(tok, dtype=jnp.int32).reshape(qblocks, QB)
    kpos = (chosen[:, :, None] * KB + jnp.arange(KB, dtype=jnp.int32)[None, None, :]).reshape(
        qblocks, span
    )
    valid = (kpos[:, None, :] <= qpos[:, :, None])[:, :, None, :]
    prob = jnp.where(valid, jnp.exp(scores - lse[..., None]), 0.0)
    prob_low = prob.astype(jnp.bfloat16)
    value_grad = give_back(
        jnp.einsum("bqgj,bqgd->bjd", prob_low, dout, preferred_element_type=jnp.float32)
    )
    value_low = value_grad.astype(jnp.bfloat16)
    all_low = lax.all_gather(value_low, XC, axis=0, tiled=True)
    me = lax.axis_index("tp")
    products = jnp.stack(
        [jnp.einsum("tf,tc->fc", p, all_low, preferred_element_type=jnp.float32) for p in planes]
    )
    order = (me - jnp.arange(tp)) % tp
    products = products[order].astype(jnp.bfloat16)
    weight_parts = to_peers(products.reshape(nz, rows_out, HD), "z")
    weight_grad = jnp.sum(weight_parts.astype(jnp.float32), axis=0)
    sel_values = fetch(values)
    dprob = jnp.einsum("bqgd,bjd->bqgj", dout, sel_values, preferred_element_type=jnp.float32)
    delta = jnp.sum(prob * dprob, axis=-1, keepdims=True)
    dscore = (prob * (dprob - delta)).astype(jnp.bfloat16)
    key_grad = give_back(
        jnp.einsum("bqgj,bqgd->bjd", dscore, query_rows, preferred_element_type=jnp.float32) * scale
    )
    query_grad = (
        jnp.einsum("bqgj,bjd->bqgd", dscore, sel_keys, preferred_element_type=jnp.float32) * scale
    )
    return (query_grad.reshape(tok, group * HD), key_grad, value_grad, weight_grad)


def solution(mesh):
    kv, tp = (mesh.shape["kv"], mesh.shape["tp"])
    split = Mesh(mesh.devices.reshape(kv // 8, 4, 2, tp), ("z", "x", "c", "tp"))
    cut = P(KV, "tp")
    return jax.shard_map(
        local,
        mesh=split,
        in_specs=(cut, cut, cut, cut, cut, cut, P(KV, None)),
        out_specs=(cut, cut, cut, cut),
        check_vma=False,
    )
```

profile of v0, /device:TPU:40, one launch (start us, length us, event | category | flops | bytes accessed | tf_op | source)
XLA Modules:
  0.0 260.3 jit_solution(17794559753755833579)
XLA Ops:
  2.1 4.3 %all-to-all-start = ((s32[8,1,16]{2,1,0:T(1,128)}), s32[8,1,16]{2,1,0:T(1,128)S(1)}, u32[]{:S(2)}, u32[]{:S(2)}) async-start(s32[8,1,16]{2,1,0:T(1,128)} %bitcast.1), calls=%async_computation | async-start | bytes 8192 | tf_op jit(solution)/shard_map/all_to_all | solution.py:16
  6.4 36.4 %all_gather.9 = bf16[2048,128]{1,0:T(8,128)(2,1)S(1)} all-gather(bf16[128,128]{1,0:T(8,128)(2,1)} %param.8), channel_id=1, replica_groups=mesh['z'=16,'x'=4,'c'=2,'tp'=4] {'z'}, dimensions={0}, use_global_device_ids=true | all-gather | bytes 557056 | tf_op jit(solution)/shard_map/all_gather | solution.py:43
  43.7 1.7 gather_fusion
  45.4 5.0 %all-to-all-start.1 = ((bf16[8,512,128]{2,1,0:T(8,128)(2,1)}), bf16[8,512,128]{2,1,0:T(8,128)(2,1)S(1)}, u32[]{:S(2)}, u32[]{:S(2)}) async-start(bf16[8,512,128]{2,1,0:T(8,128)(2,1)} %bitcast.4), calls=%async_computation.1 | async-start | bytes 2097152 | tf_op jit(solution)/shard_map/all_to_all | solution.py:16
  52.4 30.9 %all_gather.10 = bf16[2048,128]{1,0:T(8,128)(2,1)S(1)} all-gather(bf16[128,128]{1,0:T(8,128)(2,1)S(1)} %copy-done.10), channel_id=1, replica_groups=mesh['z'=16,'x'=4,'c'=2,'tp'=4] {'z'}, dimensions={0}, use_global_device_ids=true | all-gather | bytes 557056 | tf_op jit(solution)/shard_map/all_gather | solution.py:43
  83.3 1.7 gather_fusion.2
  84.9 4.8 %all-to-all-start.2 = ((bf16[8,512,128]{2,1,0:T(8,128)(2,1)}), bf16[8,512,128]{2,1,0:T(8,128)(2,1)S(1)}, u32[]{:S(2)}, u32[]{:S(2)}) async-start(bf16[8,512,128]{2,1,0:T(8,128)(2,1)} %bitcast.13), calls=%async_computation.2 | async-start | bytes 2097152 | tf_op jit(solution)/shard_map/all_to_all | solution.py:16
  89.9 1.1 pad_maximum_fusion
  91.0 1.8 gather_fusion.1
  92.8 12.8 %all-to-all-done.2 = bf16[8,512,128]{2,1,0:T(8,128)(2,1)S(1)} async-done(((bf16[8,512,128]{2,1,0:T(8,128)(2,1)}), bf16[8,512,128]{2,1,0:T(8,128)(2,1)S(1)}, u32[]{:S(2)}, u32[]{:S(2)}) %all-to-all-start.2) | async-done | bytes 1048608 | tf_op jit(solution)/shard_map/all_to_all | solution.py:16
  105.6 4.1 %all-to-all-start.7 = ((bf16[8,128,128]{1,2,0:T(8,128)(2,1)}), bf16[8,128,128]{1,2,0:T(8,128)(2,1)}, u32[]{:S(2)}, u32[]{:S(2)}) async-start(bf16[8,128,128]{1,2,0:T(8,128)(2,1)} %bitcast.27), calls=%async_computation.7 | async-start | bytes 524288 | tf_op jit(solution)/shard_map/all_to_all | solution.py:16
  110.9 0.8 fusion
  111.7 1.3 copy-done
  113.7 1.1 fusion.13
  114.8 1.4 copy-done.2
  116.3 1.3 reshape.289
  117.6 4.7 %all-to-all-start.5 = ((bf16[8,512,128]{2,1,0:T(8,128)(2,1)}), bf16[8,512,128]{2,1,0:T(8,128)(2,1)S(1)}, u32[]{:S(2)}, u32[]{:S(2)}) async-start(bf16[8,512,128]{2,1,0:T(8,128)(2,1)} %reshape.289), calls=%async_computation.5 | async-start | bytes 2097152 | tf_op jit(solution)/shard_map/all_to_all | solution.py:16
  122.3 1.8 fusion.2
  124.2 1.0 copy-done.3
  125.7 0.9 reshape.282
  126.6 2.2 fusion.14
  128.8 1.3 slice.35
  130.1 2.4 reshape.284
  132.4 5.8 %all-to-all-done.5 = bf16[8,512,128]{2,1,0:T(8,128)(2,1)S(1)} async-done(((bf16[8,512,128]{2,1,0:T(8,128)(2,1)}), bf16[8,512,128]{2,1,0:T(8,128)(2,1)S(1)}, u32[]{:S(2)}, u32[]{:S(2)}) %all-to-all-start.5) | async-done | bytes 1048608 | tf_op jit(solution)/shard_map/all_to_all | solution.py:16
  138.3 4.2 %all-to-all-start.3 = ((bf16[8,512,128]{2,1,0:T(8,128)(2,1)}), bf16[8,512,128]{2,1,0:T(8,128)(2,1)}, u32[]{:S(2)}, u32[]{:S(2)}) async-start(bf16[8,512,128]{2,1,0:T(8,128)(2,1)} %reshape.284), calls=%async_computation.3 | async-start | bytes 2097152 | tf_op jit(solution)/shard_map/all_to_all | solution.py:16
  142.6 1.3 reshape.290
  143.9 2.5 convolution_convert_fusion
  146.4 1.4 reshape.291
  147.8 10.7 %all-to-all-done.3 = bf16[8,512,128]{2,1,0:T(8,128)(2,1)} async-done(((bf16[8,512,128]{2,1,0:T(8,128)(2,1)}), bf16[8,512,128]{2,1,0:T(8,128)(2,1)}, u32[]{:S(2)}, u32[]{:S(2)}) %all-to-all-start.3) | async-done | bytes 1048608 | tf_op jit(solution)/shard_map/all_to_all | solution.py:16
  158.4 7.7 %all-to-all-start.6 = ((bf16[16,128,128]{2,1,0:T(8,128)(2,1)}), bf16[16,128,128]{2,1,0:T(8,128)(2,1)}, u32[]{:S(2)}, u32[]{:S(2)}) async-start(bf16[16,128,128]{2,1,0:T(8,128)(2,1)} %reshape.291), calls=%async_computation.6 | async-start | bytes 1048576 | tf_op jit(solution)/shard_map/all_to_all | solution.py:16
  166.2 1.5 reshape.285
  167.7 2.1 convolution_convert_fusion.1
  169.8 2.4 reshape.286
  172.2 21.9 %all-to-all-done.6 = bf16[16,128,128]{2,1,0:T(8,128)(2,1)} async-done(((bf16[16,128,128]{2,1,0:T(8,128)(2,1)}), bf16[16,128,128]{2,1,0:T(8,128)(2,1)}, u32[]{:S(2)}, u32[]{:S(2)}) %all-to-all-start.6) | async-done | bytes 524320 | tf_op jit(solution)/shard_map/all_to_all | solution.py:16
  194.1 7.3 %all-to-all-start.4 = ((bf16[16,128,128]{2,1,0:T(8,128)(2,1)}), bf16[16,128,128]{2,1,0:T(8,128)(2,1)S(1)}, u32[]{:S(2)}, u32[]{:S(2)}) async-start(bf16[16,128,128]{2,1,0:T(8,128)(2,1)} %reshape.286), calls=%async_computation.4 | async-start | bytes 1048576 | tf_op jit(solution)/shard_map/all_to_all | solution.py:16
  201.4 1.1 copy.71
  202.5 2.4 collective-permute-start.2
  204.9 4.5 %collective-permute-start.1 = (bf16[1024,128]{1,0:T(8,128)(2,1)S(1)}, bf16[1024,128]{1,0:T(8,128)(2,1)}, u32[]{:S(2)}, u32[]{:S(2)}) collective-permute-start(bf16[1024,128]{1,0:T(8,128)(2,1)S(1)} %bitcast.110), channel_id=1, source_target_pairs={{0,2},{1,3},{2,0},{3,1},{4,6},{5,7},{6,4},{7,5},{8,10},{9,11},{10,... | collective-permute-start | bytes 786440 | tf_op jit(solution)/shard_map/ppermute | solution.py:75
  209.4 3.8 %collective-permute-start = (bf16[1024,128]{1,0:T(8,128)(2,1)S(1)}, bf16[1024,128]{1,0:T(8,128)(2,1)}, u32[]{:S(2)}, u32[]{:S(2)}) collective-permute-start(bf16[1024,128]{1,0:T(8,128)(2,1)S(1)} %bitcast.111), channel_id=1, source_target_pairs={{0,1},{1,2},{2,3},{3,0},{4,5},{5,6},{6,7},{7,4},{8,9},{9,10},{10,1... | collective-permute-start | bytes 786440 | tf_op jit(solution)/shard_map/ppermute | solution.py:75
  213.3 1.1 convert_reduce_fusion
  215.0 12.8 %all_gather.11 = bf16[1024,128]{1,0:T(8,128)(2,1)S(1)} all-gather(bf16[128,128]{1,0:T(8,128)(2,1)S(1)} %get-tuple-element.4), channel_id=1, replica_groups=mesh['z'=16,'x'=4,'c'=2,'tp'=4] {'x','c'}, dimensions={0}, use_global_device_ids=true | all-gather | bytes 294912 | tf_op jit(solution)/shard_map/all_gather | solution.py:95
  228.2 1.2 convolution_bitcast_fusion.2
  229.4 1.2 convolution_bitcast_fusion.3
  230.6 1.2 convolution_bitcast_fusion.4
  233.2 12.0 %all-to-all-start.8 = ((bf16[16,32,128]{2,1,0:T(8,128)(2,1)}), bf16[16,32,128]{2,1,0:T(8,128)(2,1)S(1)}, u32[]{:S(2)}, u32[]{:S(2)}) async-start(bf16[16,32,128]{2,1,0:T(8,128)(2,1)} %bitcast.38), calls=%async_computation.8 | async-start | bytes 262144 | tf_op jit(solution)/shard_map/all_to_all | solution.py:16
  245.3 2.0 convolution_multiply_fusion
  247.3 0.9 copy.97
  248.9 10.7 %all-to-all-done.8 = bf16[16,32,128]{2,1,0:T(8,128)(2,1)S(1)} async-done(((bf16[16,32,128]{2,1,0:T(8,128)(2,1)}), bf16[16,32,128]{2,1,0:T(8,128)(2,1)S(1)}, u32[]{:S(2)}, u32[]{:S(2)}) %all-to-all-start.8) | async-done | bytes 131104 | tf_op jit(solution)/shard_map/all_to_all | solution.py:16
  (83 shorter events, 10.7 us)
Async XLA Ops:
  2.1 40.8 %all-to-all-start = ((s32[8,1,16]{2,1,0:T(1,128)}), s32[8,1,16]{2,1,0:T(1,128)S(1)}, u32[]{:S(2)}, u32[]{:S(2)}) async-start(s32[8,1,16]{2,1,0:T(1,128)} %bitcast.1), calls=%async_computation | async-start | bytes 8192 | tf_op jit(solution)/shard_map/all_to_all | solution.py:16
  43.6 7.4 %copy-start.6 = (bf16[128,1024]{1,0:T(8,128)(2,1)S(1)}, bf16[128,1024]{1,0:T(8,128)(2,1)}, u32[]{:S(2)}) copy-start(bf16[128,1024]{1,0:T(8,128)(2,1)} %param.11) | copy-start | bytes 786436
  43.6 7.4 %copy-start.12 = (f32[128,8]{0,1:T(8,128)S(1)}, f32[128,8]{0,1:T(8,128)}, u32[]{:S(2)}) copy-start(f32[128,8]{0,1:T(8,128)} %param.10) | copy-start | bytes 12292
  43.6 7.5 %copy-start.7 = (bf16[128,1024]{1,0:T(8,128)(2,1)S(1)}, bf16[128,1024]{1,0:T(8,128)(2,1)}, u32[]{:S(2)}) copy-start(bf16[128,1024]{1,0:T(8,128)(2,1)} %param.7) | copy-start | bytes 786436
  45.4 6.1 %copy-start.8 = (bf16[128,1024]{1,0:T(8,128)(2,1)S(1)}, bf16[128,1024]{1,0:T(8,128)(2,1)}, u32[]{:S(2)}) copy-start(bf16[128,1024]{1,0:T(8,128)(2,1)} %param.12) | copy-start | bytes 786436
  45.4 7.0 %copy-start.10 = (bf16[128,128]{1,0:T(8,128)(2,1)S(1)}, bf16[128,128]{1,0:T(8,128)(2,1)}, u32[]{:S(2)}) copy-start(bf16[128,128]{1,0:T(8,128)(2,1)} %param.9) | copy-start | bytes 98308
  45.4 39.6 %all-to-all-start.1 = ((bf16[8,512,128]{2,1,0:T(8,128)(2,1)}), bf16[8,512,128]{2,1,0:T(8,128)(2,1)S(1)}, u32[]{:S(2)}, u32[]{:S(2)}) async-start(bf16[8,512,128]{2,1,0:T(8,128)(2,1)} %bitcast.4), calls=%async_computation.1 | async-start | bytes 2097152 | tf_op jit(solution)/shard_map/all_to_all | solution.py:16
  83.3 6.6 %copy-start.9 = (bf16[128,128]{1,0:T(8,128)(2,1)S(1)}, bf16[128,128]{1,0:T(8,128)(2,1)}, u32[]{:S(2)}) copy-start(bf16[128,128]{1,0:T(8,128)(2,1)} %param.8) | copy-start | bytes 98308
  84.9 20.7 %all-to-all-start.2 = ((bf16[8,512,128]{2,1,0:T(8,128)(2,1)}), bf16[8,512,128]{2,1,0:T(8,128)(2,1)S(1)}, u32[]{:S(2)}, u32[]{:S(2)}) async-start(bf16[8,512,128]{2,1,0:T(8,128)(2,1)} %bitcast.13), calls=%async_computation.2 | async-start | bytes 2097152 | tf_op jit(solution)/shard_map/all_to_all | solution.py:16
  92.8 18.0 %copy-start.4 = (bf16[32,32,128]{2,1,0:T(8,128)(2,1)}, bf16[32,32,128]{2,1,0:T(8,128)(2,1)S(1)}, u32[]{:S(2)}) copy-start(bf16[32,32,128]{2,1,0:T(8,128)(2,1)S(1)} %gather_fusion.1) | copy-start | bytes 786436
  105.6 12.0 %all-to-all-start.7 = ((bf16[8,128,128]{1,2,0:T(8,128)(2,1)}), bf16[8,128,128]{1,2,0:T(8,128)(2,1)}, u32[]{:S(2)}, u32[]{:S(2)}) async-start(bf16[8,128,128]{1,2,0:T(8,128)(2,1)} %bitcast.27), calls=%async_computation.7 | async-start | bytes 524288 | tf_op jit(solution)/shard_map/all_to_all | solution.py:16
  111.7 1.3 copy-start
  111.7 2.0 copy-start.13
  114.8 1.4 copy-start.2
  117.6 20.6 %all-to-all-start.5 = ((bf16[8,512,128]{2,1,0:T(8,128)(2,1)}), bf16[8,512,128]{2,1,0:T(8,128)(2,1)S(1)}, u32[]{:S(2)}, u32[]{:S(2)}) async-start(bf16[8,512,128]{2,1,0:T(8,128)(2,1)} %reshape.289), calls=%async_computation.5 | async-start | bytes 2097152 | tf_op jit(solution)/shard_map/all_to_all | solution.py:16
  124.2 1.0 copy-start.3
  128.8 116.5 %copy-start.1 = (f32[132,4096]{1,0:T(8,128)}, f32[132,4096]{1,0:T(8,128)S(1)}, u32[]{:S(2)}) copy-start(f32[132,4096]{1,0:T(8,128)S(1)} %fusion.14) | copy-start | bytes 6488068
  130.1 12.4 %copy-start.11 = (s32[8,16]{1,0:T(8,128)S(1)}, s32[8,16]{1,0:T(8,128)}, u32[]{:S(2)}) copy-start(s32[8,16]{1,0:T(8,128)} %get-tuple-element.9) | copy-start | bytes 1540
  138.3 20.2 %all-to-all-start.3 = ((bf16[8,512,128]{2,1,0:T(8,128)(2,1)}), bf16[8,512,128]{2,1,0:T(8,128)(2,1)}, u32[]{:S(2)}, u32[]{:S(2)}) async-start(bf16[8,512,128]{2,1,0:T(8,128)(2,1)} %reshape.284), calls=%async_computation.3 | async-start | bytes 2097152 | tf_op jit(solution)/shard_map/all_to_all | solution.py:16
  158.4 35.6 %all-to-all-start.6 = ((bf16[16,128,128]{2,1,0:T(8,128)(2,1)}), bf16[16,128,128]{2,1,0:T(8,128)(2,1)}, u32[]{:S(2)}, u32[]{:S(2)}) async-start(bf16[16,128,128]{2,1,0:T(8,128)(2,1)} %reshape.291), calls=%async_computation.6 | async-start | bytes 1048576 | tf_op jit(solution)/shard_map/all_to_all | solution.py:16
  167.7 45.5 %slice-start.1 = ((f32[132,4096]{1,0:T(8,128)}), f32[4,4096]{1,0:T(4,128)S(1)}, s32[]{:S(2)}) async-start(f32[132,4096]{1,0:T(8,128)} %copy-done.2), calls=%async_computation.10 | async-start | bytes 131072 | tf_op jit(solution)/shard_map/slice | solution.py:60
  194.1 39.2 %all-to-all-start.4 = ((bf16[16,128,128]{2,1,0:T(8,128)(2,1)}), bf16[16,128,128]{2,1,0:T(8,128)(2,1)S(1)}, u32[]{:S(2)}, u32[]{:S(2)}) async-start(bf16[16,128,128]{2,1,0:T(8,128)(2,1)} %reshape.286), calls=%async_computation.4 | async-start | bytes 1048576 | tf_op jit(solution)/shard_map/all_to_all | solution.py:16
  202.5 25.6 %collective-permute-start.2 = (bf16[1024,128]{1,0:T(8,128)(2,1)S(1)}, bf16[1024,128]{1,0:T(8,128)(2,1)}, u32[]{:S(2)}, u32[]{:S(2)}) collective-permute-start(bf16[1024,128]{1,0:T(8,128)(2,1)S(1)} %bitcast.109), channel_id=1, source_target_pairs={{0,3},{1,0},{2,1},{3,2},{4,7},{5,4},{6,5},{7,6},{8,11},{9,8},{10,9... | collective-permute-start | bytes 786440 | tf_op jit(solution)/shard_map/ppermute | solution.py:75
  204.9 24.5 %collective-permute-start.1 = (bf16[1024,128]{1,0:T(8,128)(2,1)S(1)}, bf16[1024,128]{1,0:T(8,128)(2,1)}, u32[]{:S(2)}, u32[]{:S(2)}) collective-permute-start(bf16[1024,128]{1,0:T(8,128)(2,1)S(1)} %bitcast.110), channel_id=1, source_target_pairs={{0,2},{1,3},{2,0},{3,1},{4,6},{5,7},{6,4},{7,5},{8,10},{9,11},{10,... | collective-permute-start | bytes 786440 | tf_op jit(solution)/shard_map/ppermute | solution.py:75
  209.4 21.2 %collective-permute-start = (bf16[1024,128]{1,0:T(8,128)(2,1)S(1)}, bf16[1024,128]{1,0:T(8,128)(2,1)}, u32[]{:S(2)}, u32[]{:S(2)}) collective-permute-start(bf16[1024,128]{1,0:T(8,128)(2,1)S(1)} %bitcast.111), channel_id=1, source_target_pairs={{0,1},{1,2},{2,3},{3,0},{4,5},{5,6},{6,7},{7,4},{8,9},{9,10},{10,1... | collective-permute-start | bytes 786440 | tf_op jit(solution)/shard_map/ppermute | solution.py:75
  214.4 30.9 %copy-start.5 = (bf16[32,32,128]{2,1,0:T(8,128)(2,1)S(1)}, bf16[32,32,128]{2,1,0:T(8,128)(2,1)}, u32[]{:S(2)}) copy-start(bf16[32,32,128]{2,1,0:T(8,128)(2,1)} %copy-done.4) | copy-start | bytes 786436
  233.2 26.4 %all-to-all-start.8 = ((bf16[16,32,128]{2,1,0:T(8,128)(2,1)}), bf16[16,32,128]{2,1,0:T(8,128)(2,1)S(1)}, u32[]{:S(2)}, u32[]{:S(2)}) async-start(bf16[16,32,128]{2,1,0:T(8,128)(2,1)} %bitcast.38), calls=%async_computation.8 | async-start | bytes 262144 | tf_op jit(solution)/shard_map/all_to_all | solution.py:16
  245.3 2.9 %slice-start = ((f32[132,4096]{1,0:T(8,128)}), f32[4,4096]{1,0:T(4,128)S(1)}, s32[]{:S(2)}) async-start(f32[132,4096]{1,0:T(8,128)} %copy-done.1), calls=%async_computation.9 | async-start | bytes 131072 | tf_op jit(solution)/shard_map/slice | solution.py:60
where the time goes:
time: 262 us; the launch traced here: 260 us
  blocking collectives  80.2 us (31%)
  starting transfers between devices  64.8 us (25%)
  waiting for transfers between devices  61.9 us (24%)
  local copies, waits for them, and re-layouts  28.5 us (11%)
  matrix products  16.1 us (6%)
  other arithmetic  7.73 us (3%)
    all_gather x2, blocking collectives, fetch(): lax.all_gather(rows, 'z', axis=0, tiled=True).reshape(nz * kblocks, KB, HD)  67.3 us
    all_to_all x9, waiting for transfers between devices, to_peers(): return lax.all_to_all(parts, axis, split_axis=0, concat_axis=0, tiled=True)  61.9 us
    all_to_all x9, starting transfers between devices, to_peers(): return lax.all_to_all(parts, axis, split_axis=0, concat_axis=0, tiled=True)  54.1 us
    all_gather x1, blocking collectives, local(): all_low = lax.all_gather(value_low, XC, axis=0, tiled=True)  12.8 us
    ppermute x3, starting transfers between devices, local(): lax.ppermute(split, 'tp', [(i, (i + k) % tp) for i in range(tp)])  10.7 us
  transfers between devices with their start and end apart: 12, of which 5 were waited for; matrix products, arithmetic and copies ran while one was open for 17% of the time, Pallas kernels for 0%

commit v1 on v0

--- a/solution.py
+++ b/solution.py
@@ -92,7 +92,9 @@
         jnp.einsum("bqgj,bqgd->bjd", prob_low, dout, preferred_element_type=jnp.float32)
     )
     value_low = value_grad.astype(jnp.bfloat16)
-    all_low = lax.all_gather(value_low, XC, axis=0, tiled=True)
+    all_low = jnp.concatenate(
+        lax.all_to_all(jnp.stack([value_low] * lax.axis_size(XC)), XC, 0, 0), axis=0
+    )
     me = lax.axis_index("tp")
     products = jnp.stack(
         [jnp.einsum("tf,tc->fc", p, all_low, preferred_element_type=jnp.float32) for p in planes]

time: 262 us -> 271 us (1.034)
  the two profiles are of different devices: /device:TPU:40 before, /device:TPU:32 now
where the time goes in v1:
time: 271 us; the launch traced here: 270 us
  waiting for transfers between devices  83.6 us (31%)
  blocking collectives  67.4 us (25%)
  starting transfers between devices  64.4 us (24%)
  local copies, waits for them, and re-layouts  28.5 us (11%)
  matrix products  17 us (6%)
  other arithmetic  7.71 us (3%)
    all_to_all x9, waiting for transfers between devices, to_peers(): return lax.all_to_all(parts, axis, split_axis=0, concat_axis=0, tiled=True)  72.8 us
    all_gather x2, blocking collectives, fetch(): lax.all_gather(rows, 'z', axis=0, tiled=True).reshape(nz * kblocks, KB, HD)  67.4 us
    all_to_all x9, starting transfers between devices, to_peers(): return lax.all_to_all(parts, axis, split_axis=0, concat_axis=0, tiled=True)  50.3 us
    ppermute x3, starting transfers between devices, local(): lax.ppermute(split, 'tp', [(i, (i + k) % tp) for i in range(tp)])  10.5 us
    ppermute x3, waiting for transfers between devices, local(): lax.ppermute(split, 'tp', [(i, (i + k) % tp) for i in range(tp)])  8.08 us
  transfers between devices with their start and end apart: 13, of which 11 were waited for; matrix products, arithmetic and copies ran while one was open for 15% of the time, Pallas kernels for 0%

profile of v1, /device:TPU:32, one launch (start us, length us, event | category | flops | bytes accessed | tf_op | source)
XLA Modules:
  0.0 269.7 jit_solution(10144061014065642791)
XLA Ops:
  2.1 4.3 %all-to-all-start = ((s32[8,1,16]{2,1,0:T(1,128)}), s32[8,1,16]{2,1,0:T(1,128)S(1)}, u32[]{:S(2)}, u32[]{:S(2)}) async-start(s32[8,1,16]{2,1,0:T(1,128)} %bitcast.1), calls=%async_computation | async-start | bytes 8192 | tf_op jit(solution)/shard_map/all_to_all | solution.py:16
  6.4 36.4 %all_gather.6 = bf16[2048,128]{1,0:T(8,128)(2,1)S(1)} all-gather(bf16[128,128]{1,0:T(8,128)(2,1)} %param.8), channel_id=1, replica_groups=mesh['z'=16,'x'=4,'c'=2,'tp'=4] {'z'}, dimensions={0}, use_global_device_ids=true | all-gather | bytes 557056 | tf_op jit(solution)/shard_map/all_gather | solution.py:43
  43.7 1.7 gather_fusion
  45.3 5.0 %all-to-all-start.1 = ((bf16[8,512,128]{2,1,0:T(8,128)(2,1)}), bf16[8,512,128]{2,1,0:T(8,128)(2,1)S(1)}, u32[]{:S(2)}, u32[]{:S(2)}) async-start(bf16[8,512,128]{2,1,0:T(8,128)(2,1)} %bitcast.4), calls=%async_computation.1 | async-start | bytes 2097152 | tf_op jit(solution)/shard_map/all_to_all | solution.py:16
  51.4 30.9 %all_gather.7 = bf16[2048,128]{1,0:T(8,128)(2,1)S(1)} all-gather(bf16[128,128]{1,0:T(8,128)(2,1)S(1)} %copy-done.10), channel_id=1, replica_groups=mesh['z'=16,'x'=4,'c'=2,'tp'=4] {'z'}, dimensions={0}, use_global_device_ids=true | all-gather | bytes 557056 | tf_op jit(solution)/shard_map/all_gather | solution.py:43
  82.4 1.7 gather_fusion.2
  84.0 4.7 %all-to-all-start.2 = ((bf16[8,512,128]{2,1,0:T(8,128)(2,1)}), bf16[8,512,128]{2,1,0:T(8,128)(2,1)S(1)}, u32[]{:S(2)}, u32[]{:S(2)}) async-start(bf16[8,512,128]{2,1,0:T(8,128)(2,1)} %bitcast.13), calls=%async_computation.2 | async-start | bytes 2097152 | tf_op jit(solution)/shard_map/all_to_all | solution.py:16
  90.0 1.8 gather_fusion.1
  91.9 12.8 %all-to-all-done.2 = bf16[8,512,128]{2,1,0:T(8,128)(2,1)S(1)} async-done(((bf16[8,512,128]{2,1,0:T(8,128)(2,1)}), bf16[8,512,128]{2,1,0:T(8,128)(2,1)S(1)}, u32[]{:S(2)}, u32[]{:S(2)}) %all-to-all-start.2) | async-done | bytes 1048608 | tf_op jit(solution)/shard_map/all_to_all | solution.py:16
  106.7 1.3 copy-done
  108.7 1.1 fusion.13
  109.9 1.4 copy-done.2
  111.4 1.3 reshape.296
  112.7 3.6 %all-to-all-start.5 = ((bf16[8,512,128]{2,1,0:T(8,128)(2,1)}), bf16[8,512,128]{2,1,0:T(8,128)(2,1)S(1)}, u32[]{:S(2)}, u32[]{:S(2)}) async-start(bf16[8,512,128]{2,1,0:T(8,128)(2,1)} %reshape.296), calls=%async_computation.5 | async-start | bytes 2097152 | tf_op jit(solution)/shard_map/all_to_all | solution.py:16
  116.2 1.8 fusion.2
  120.5 2.2 fusion.14
  122.7 1.3 slice.35
  124.0 2.3 reshape.291
  126.4 5.7 %all-to-all-done.5 = bf16[8,512,128]{2,1,0:T(8,128)(2,1)S(1)} async-done(((bf16[8,512,128]{2,1,0:T(8,128)(2,1)}), bf16[8,512,128]{2,1,0:T(8,128)(2,1)S(1)}, u32[]{:S(2)}, u32[]{:S(2)}) %all-to-all-start.5) | async-done | bytes 1048608 | tf_op jit(solution)/shard_map/all_to_all | solution.py:16
  132.1 4.3 %all-to-all-start.3 = ((bf16[8,512,128]{2,1,0:T(8,128)(2,1)}), bf16[8,512,128]{2,1,0:T(8,128)(2,1)}, u32[]{:S(2)}, u32[]{:S(2)}) async-start(bf16[8,512,128]{2,1,0:T(8,128)(2,1)} %reshape.291), calls=%async_computation.3 | async-start | bytes 2097152 | tf_op jit(solution)/shard_map/all_to_all | solution.py:16
  136.4 1.3 reshape.297
  137.7 2.6 convolution_convert_fusion
  140.3 1.3 reshape.298
  141.6 10.7 %all-to-all-done.3 = bf16[8,512,128]{2,1,0:T(8,128)(2,1)} async-done(((bf16[8,512,128]{2,1,0:T(8,128)(2,1)}), bf16[8,512,128]{2,1,0:T(8,128)(2,1)}, u32[]{:S(2)}, u32[]{:S(2)}) %all-to-all-start.3) | async-done | bytes 1048608 | tf_op jit(solution)/shard_map/all_to_all | solution.py:16
  152.3 7.7 %all-to-all-start.6 = ((bf16[16,128,128]{2,1,0:T(8,128)(2,1)}), bf16[16,128,128]{2,1,0:T(8,128)(2,1)}, u32[]{:S(2)}, u32[]{:S(2)}) async-start(bf16[16,128,128]{2,1,0:T(8,128)(2,1)} %reshape.298), calls=%async_computation.6 | async-start | bytes 1048576 | tf_op jit(solution)/shard_map/all_to_all | solution.py:16
  161.1 1.5 reshape.292
  162.6 25.3 %all-to-all-done.6 = bf16[16,128,128]{2,1,0:T(8,128)(2,1)} async-done(((bf16[16,128,128]{2,1,0:T(8,128)(2,1)}), bf16[16,128,128]{2,1,0:T(8,128)(2,1)}, u32[]{:S(2)}, u32[]{:S(2)}) %all-to-all-start.6) | async-done | bytes 524320 | tf_op jit(solution)/shard_map/all_to_all | solution.py:16
  187.9 4.1 %all-to-all-start.8 = ((bf16[8,128,128]{2,1,0:T(8,128)(2,1)}), bf16[8,128,128]{2,1,0:T(8,128)(2,1)}, u32[]{:S(2)}, u32[]{:S(2)}) async-start(bf16[8,128,128]{2,1,0:T(8,128)(2,1)} %copy.66), calls=%async_computation.8 | async-start | bytes 524288 | tf_op jit(solution)/shard_map/all_to_all | solution.py:16
  193.8 5.6 %all-to-all-done.8 = bf16[8,128,128]{2,1,0:T(8,128)(2,1)} async-done(((bf16[8,128,128]{2,1,0:T(8,128)(2,1)}), bf16[8,128,128]{2,1,0:T(8,128)(2,1)}, u32[]{:S(2)}, u32[]{:S(2)}) %all-to-all-start.8) | async-done | bytes 262176 | tf_op jit(solution)/shard_map/all_to_all | solution.py:16
  200.2 3.6 %all-to-all-start.7 = ((bf16[8,128,128]{1,2,0:T(8,128)(2,1)}), bf16[8,128,128]{1,2,0:T(8,128)(2,1)S(1)}, u32[]{:S(2)}, u32[]{:S(2)}) async-start(bf16[8,128,128]{1,2,0:T(8,128)(2,1)} %stack.12), calls=%async_computation.7 | async-start | bytes 524288 | tf_op jit(solution)/shard_map/all_to_all | solution.py:96
  203.8 2.1 convolution_convert_fusion.1
  205.9 2.4 reshape.293
  208.3 2.8 %all-to-all-done.7 = bf16[8,128,128]{1,2,0:T(8,128)(2,1)S(1)} async-done(((bf16[8,128,128]{1,2,0:T(8,128)(2,1)}), bf16[8,128,128]{1,2,0:T(8,128)(2,1)S(1)}, u32[]{:S(2)}, u32[]{:S(2)}) %all-to-all-start.7) | async-done | bytes 262176 | tf_op jit(solution)/shard_map/all_to_all | solution.py:96
  211.1 7.3 %all-to-all-start.4 = ((bf16[16,128,128]{2,1,0:T(8,128)(2,1)}), bf16[16,128,128]{2,1,0:T(8,128)(2,1)S(1)}, u32[]{:S(2)}, u32[]{:S(2)}) async-start(bf16[16,128,128]{2,1,0:T(8,128)(2,1)} %reshape.293), calls=%async_computation.4 | async-start | bytes 1048576 | tf_op jit(solution)/shard_map/all_to_all | solution.py:16
  218.4 5.1 %collective-permute-start.2 = (bf16[1024,128]{1,0:T(8,128)(2,1)}, bf16[1024,128]{1,0:T(8,128)(2,1)}, u32[]{:S(2)}, u32[]{:S(2)}) collective-permute-start(bf16[1024,128]{1,0:T(8,128)(2,1)} %bitcast.32), channel_id=1, source_target_pairs={{0,3},{1,0},{2,1},{3,2},{4,7},{5,4},{6,5},{7,6},{8,11},{9,8},{10,9... | collective-permute-start | bytes 786440 | tf_op jit(solution)/shard_map/ppermute | solution.py:75
  223.4 2.5 collective-permute-start.1
  226.0 2.9 %collective-permute-start = (bf16[1024,128]{1,0:T(8,128)(2,1)}, bf16[1024,128]{1,0:T(8,128)(2,1)}, u32[]{:S(2)}, u32[]{:S(2)}) collective-permute-start(bf16[1024,128]{1,0:T(8,128)(2,1)} %bitcast.32), channel_id=1, source_target_pairs={{0,1},{1,2},{2,3},{3,0},{4,5},{5,6},{6,7},{7,4},{8,9},{9,10},{10,1... | collective-permute-start | bytes 786440 | tf_op jit(solution)/shard_map/ppermute | solution.py:75
  229.1 4.9 %collective-permute-done.2 = bf16[1024,128]{1,0:T(8,128)(2,1)} collective-permute-done((bf16[1024,128]{1,0:T(8,128)(2,1)}, bf16[1024,128]{1,0:T(8,128)(2,1)}, u32[]{:S(2)}, u32[]{:S(2)}) %collective-permute-start.2) | collective-permute-done | bytes 262176 | tf_op jit(solution)/shard_map/ppermute | solution.py:75
  234.0 1.2 convolution_bitcast_fusion.2
  235.2 1.1 collective-permute-done.1
  236.3 1.2 convolution_bitcast_fusion.3
  237.6 2.1 collective-permute-done
  239.6 1.2 convolution_bitcast_fusion.4
  240.8 1.2 convolution_bitcast_fusion.5
  243.4 2.6 all-to-all-done.4
  246.0 9.4 %all-to-all-start.9 = ((bf16[16,32,128]{2,1,0:T(8,128)(2,1)}), bf16[16,32,128]{2,1,0:T(8,128)(2,1)S(1)}, u32[]{:S(2)}, u32[]{:S(2)}) async-start(bf16[16,32,128]{2,1,0:T(8,128)(2,1)} %bitcast.40), calls=%async_computation.9 | async-start | bytes 262144 | tf_op jit(solution)/shard_map/all_to_all | solution.py:16
  255.4 1.9 convolution_multiply_fusion
  259.1 10.0 %all-to-all-done.9 = bf16[16,32,128]{2,1,0:T(8,128)(2,1)S(1)} async-done(((bf16[16,32,128]{2,1,0:T(8,128)(2,1)}), bf16[16,32,128]{2,1,0:T(8,128)(2,1)S(1)}, u32[]{:S(2)}, u32[]{:S(2)}) %all-to-all-start.9) | async-done | bytes 131104 | tf_op jit(solution)/shard_map/all_to_all | solution.py:16
  (87 shorter events, 17.3 us)
Async XLA Ops:
  2.1 40.8 %all-to-all-start = ((s32[8,1,16]{2,1,0:T(1,128)}), s32[8,1,16]{2,1,0:T(1,128)S(1)}, u32[]{:S(2)}, u32[]{:S(2)}) async-start(s32[8,1,16]{2,1,0:T(1,128)} %bitcast.1), calls=%async_computation | async-start | bytes 8192 | tf_op jit(solution)/shard_map/all_to_all | solution.py:16
  43.6 7.4 %copy-start.6 = (bf16[128,1024]{1,0:T(8,128)(2,1)S(1)}, bf16[128,1024]{1,0:T(8,128)(2,1)}, u32[]{:S(2)}) copy-start(bf16[128,1024]{1,0:T(8,128)(2,1)} %param.11) | copy-start | bytes 786436
  43.6 7.4 %copy-start.12 = (f32[128,8]{0,1:T(8,128)S(1)}, f32[128,8]{0,1:T(8,128)}, u32[]{:S(2)}) copy-start(f32[128,8]{0,1:T(8,128)} %param.10) | copy-start | bytes 12292
  43.6 7.5 %copy-start.7 = (bf16[128,1024]{1,0:T(8,128)(2,1)S(1)}, bf16[128,1024]{1,0:T(8,128)(2,1)}, u32[]{:S(2)}) copy-start(bf16[128,1024]{1,0:T(8,128)(2,1)} %param.7) | copy-start | bytes 786436
  45.3 6.1 %copy-start.10 = (bf16[128,128]{1,0:T(8,128)(2,1)S(1)}, bf16[128,128]{1,0:T(8,128)(2,1)}, u32[]{:S(2)}) copy-start(bf16[128,128]{1,0:T(8,128)(2,1)} %param.9) | copy-start | bytes 98308
  45.3 38.7 %all-to-all-start.1 = ((bf16[8,512,128]{2,1,0:T(8,128)(2,1)}), bf16[8,512,128]{2,1,0:T(8,128)(2,1)S(1)}, u32[]{:S(2)}, u32[]{:S(2)}) async-start(bf16[8,512,128]{2,1,0:T(8,128)(2,1)} %bitcast.4), calls=%async_computation.1 | async-start | bytes 2097152 | tf_op jit(solution)/shard_map/all_to_all | solution.py:16
  82.4 6.5 %copy-start.9 = (bf16[128,128]{1,0:T(8,128)(2,1)S(1)}, bf16[128,128]{1,0:T(8,128)(2,1)}, u32[]{:S(2)}) copy-start(bf16[128,128]{1,0:T(8,128)(2,1)} %param.8) | copy-start | bytes 98308
  84.0 20.7 %all-to-all-start.2 = ((bf16[8,512,128]{2,1,0:T(8,128)(2,1)}), bf16[8,512,128]{2,1,0:T(8,128)(2,1)S(1)}, u32[]{:S(2)}, u32[]{:S(2)}) async-start(bf16[8,512,128]{2,1,0:T(8,128)(2,1)} %bitcast.13), calls=%async_computation.2 | async-start | bytes 2097152 | tf_op jit(solution)/shard_map/all_to_all | solution.py:16
  91.9 14.0 %copy-start.4 = (bf16[32,32,128]{2,1,0:T(8,128)(2,1)}, bf16[32,32,128]{2,1,0:T(8,128)(2,1)S(1)}, u32[]{:S(2)}) copy-start(bf16[32,32,128]{2,1,0:T(8,128)(2,1)S(1)} %gather_fusion.1) | copy-start | bytes 786436
  106.7 1.4 copy-start
  106.7 2.0 copy-start.13
  109.9 1.4 copy-start.2
  112.7 19.4 %all-to-all-start.5 = ((bf16[8,512,128]{2,1,0:T(8,128)(2,1)}), bf16[8,512,128]{2,1,0:T(8,128)(2,1)S(1)}, u32[]{:S(2)}, u32[]{:S(2)}) async-start(bf16[8,512,128]{2,1,0:T(8,128)(2,1)} %reshape.296), calls=%async_computation.5 | async-start | bytes 2097152 | tf_op jit(solution)/shard_map/all_to_all | solution.py:16
  118.1 1.0 copy-start.3
  122.7 132.7 %copy-start.1 = (f32[132,4096]{1,0:T(8,128)}, f32[132,4096]{1,0:T(8,128)S(1)}, u32[]{:S(2)}) copy-start(f32[132,4096]{1,0:T(8,128)S(1)} %fusion.14) | copy-start | bytes 6488068
  124.0 12.3 %copy-start.11 = (s32[8,16]{1,0:T(8,128)S(1)}, s32[8,16]{1,0:T(8,128)}, u32[]{:S(2)}) copy-start(s32[8,16]{1,0:T(8,128)} %get-tuple-element.9) | copy-start | bytes 1540
  132.1 20.2 %all-to-all-start.3 = ((bf16[8,512,128]{2,1,0:T(8,128)(2,1)}), bf16[8,512,128]{2,1,0:T(8,128)(2,1)}, u32[]{:S(2)}, u32[]{:S(2)}) async-start(bf16[8,512,128]{2,1,0:T(8,128)(2,1)} %reshape.291), calls=%async_computation.3 | async-start | bytes 2097152 | tf_op jit(solution)/shard_map/all_to_all | solution.py:16
  137.7 22.3 %copy-start.8 = (bf16[128,1024]{1,0:T(8,128)(2,1)S(1)}, bf16[128,1024]{1,0:T(8,128)(2,1)}, u32[]{:S(2)}) copy-start(bf16[128,1024]{1,0:T(8,128)(2,1)} %param.12) | copy-start | bytes 786436
  140.3 20.8 %slice-start.1 = ((f32[132,4096]{1,0:T(8,128)}), f32[4,4096]{1,0:T(4,128)S(1)}, s32[]{:S(2)}) async-start(f32[132,4096]{1,0:T(8,128)} %copy-done.2), calls=%async_computation.11 | async-start | bytes 131072 | tf_op jit(solution)/shard_map/slice | solution.py:60
  152.3 35.6 %all-to-all-start.6 = ((bf16[16,128,128]{2,1,0:T(8,128)(2,1)}), bf16[16,128,128]{2,1,0:T(8,128)(2,1)}, u32[]{:S(2)}, u32[]{:S(2)}) async-start(bf16[16,128,128]{2,1,0:T(8,128)(2,1)} %reshape.298), calls=%async_computation.6 | async-start | bytes 1048576 | tf_op jit(solution)/shard_map/all_to_all | solution.py:16
  187.9 11.6 %all-to-all-start.8 = ((bf16[8,128,128]{2,1,0:T(8,128)(2,1)}), bf16[8,128,128]{2,1,0:T(8,128)(2,1)}, u32[]{:S(2)}, u32[]{:S(2)}) async-start(bf16[8,128,128]{2,1,0:T(8,128)(2,1)} %copy.66), calls=%async_computation.8 | async-start | bytes 524288 | tf_op jit(solution)/shard_map/all_to_all | solution.py:16
  200.2 10.8 %all-to-all-start.7 = ((bf16[8,128,128]{1,2,0:T(8,128)(2,1)}), bf16[8,128,128]{1,2,0:T(8,128)(2,1)S(1)}, u32[]{:S(2)}, u32[]{:S(2)}) async-start(bf16[8,128,128]{1,2,0:T(8,128)(2,1)} %stack.12), calls=%async_computation.7 | async-start | bytes 524288 | tf_op jit(solution)/shard_map/all_to_all | solution.py:96
  211.1 34.9 %all-to-all-start.4 = ((bf16[16,128,128]{2,1,0:T(8,128)(2,1)}), bf16[16,128,128]{2,1,0:T(8,128)(2,1)S(1)}, u32[]{:S(2)}, u32[]{:S(2)}) async-start(bf16[16,128,128]{2,1,0:T(8,128)(2,1)} %reshape.293), calls=%async_computation.4 | async-start | bytes 1048576 | tf_op jit(solution)/shard_map/all_to_all | solution.py:16
  218.4 37.1 %copy-start.5 = (bf16[32,32,128]{2,1,0:T(8,128)(2,1)S(1)}, bf16[32,32,128]{2,1,0:T(8,128)(2,1)}, u32[]{:S(2)}) copy-start(bf16[32,32,128]{2,1,0:T(8,128)(2,1)} %copy-done.4) | copy-start | bytes 786436
  218.4 15.6 %collective-permute-start.2 = (bf16[1024,128]{1,0:T(8,128)(2,1)}, bf16[1024,128]{1,0:T(8,128)(2,1)}, u32[]{:S(2)}, u32[]{:S(2)}) collective-permute-start(bf16[1024,128]{1,0:T(8,128)(2,1)} %bitcast.32), channel_id=1, source_target_pairs={{0,3},{1,0},{2,1},{3,2},{4,7},{5,4},{6,5},{7,6},{8,11},{9,8},{10,9... | collective-permute-start | bytes 786440 | tf_op jit(solution)/shard_map/ppermute | solution.py:75
  223.4 12.9 %collective-permute-start.1 = (bf16[1024,128]{1,0:T(8,128)(2,1)}, bf16[1024,128]{1,0:T(8,128)(2,1)}, u32[]{:S(2)}, u32[]{:S(2)}) collective-permute-start(bf16[1024,128]{1,0:T(8,128)(2,1)} %bitcast.32), channel_id=1, source_target_pairs={{0,2},{1,3},{2,0},{3,1},{4,6},{5,7},{6,4},{7,5},{8,10},{9,11},{10,... | collective-permute-start | bytes 786440 | tf_op jit(solution)/shard_map/ppermute | solution.py:75
  226.0 13.6 %collective-permute-start = (bf16[1024,128]{1,0:T(8,128)(2,1)}, bf16[1024,128]{1,0:T(8,128)(2,1)}, u32[]{:S(2)}, u32[]{:S(2)}) collective-permute-start(bf16[1024,128]{1,0:T(8,128)(2,1)} %bitcast.32), channel_id=1, source_target_pairs={{0,1},{1,2},{2,3},{3,0},{4,5},{5,6},{6,7},{7,4},{8,9},{9,10},{10,1... | collective-permute-start | bytes 786440 | tf_op jit(solution)/shard_map/ppermute | solution.py:75
  246.0 23.1 %all-to-all-start.9 = ((bf16[16,32,128]{2,1,0:T(8,128)(2,1)}), bf16[16,32,128]{2,1,0:T(8,128)(2,1)S(1)}, u32[]{:S(2)}, u32[]{:S(2)}) async-start(bf16[16,32,128]{2,1,0:T(8,128)(2,1)} %bitcast.40), calls=%async_computation.9 | async-start | bytes 262144 | tf_op jit(solution)/shard_map/all_to_all | solution.py:16
  255.4 2.9 %slice-start = ((f32[132,4096]{1,0:T(8,128)}), f32[4,4096]{1,0:T(4,128)S(1)}, s32[]{:S(2)}) async-start(f32[132,4096]{1,0:T(8,128)} %copy-done.1), calls=%async_computation.10 | async-start | bytes 131072 | tf_op jit(solution)/shard_map/slice | solution.py:60
